TPU v7x, 512 devices: a whole 4x8x8 slice. The times are simulated.
512 devices in a mesh: row: 32 (over z, x), col: 16 (over y, core).
Axes of the slice: x: 4, y: 8, z: 8, core: 2. Of those that a mesh axis runs over, the one named last changes fastest.
Arguments:
- tokens: bfloat16 [32768, 2048], P('row'), may hold values from -136 to 136
- norm_gain: float32 [2048], replicated, may hold values from 0.1 to 1.9
- w_in: bfloat16 [2048, 1024], P(None, 'col'), may hold values from -0.125 to 0.125
- w_out: bfloat16 [1024, 2048], P(None, 'col'), may hold values from -0.1875 to 0.1875
Outputs:
- mixed_tokens: bfloat16 [32768, 2048], P('row', 'col')
All inputs are finite; a program needn't handle non-finite values.
Results may differ from a plain program's by a relative error of at most 0.013.
Values may be sent and summed in bfloat16 or wider, within the bound.
No kernel may reach another device: no remote copies, remote signals or barrier semaphores. Data moves between devices by JAX's collectives and lax.ppermute only.
A program may use at most 64 MiB of HBM per device.

v0:
```python
import math

import jax
import jax.numpy as jnp
import numpy as np
from jax import lax
from jax.experimental import pallas as pl
from jax.experimental.pallas import tpu as pltpu
from jax.sharding import Mesh
from jax.sharding import PartitionSpec as P


GROUP = 256
NORM_EPS = 1e-06
BLOCK = 128
AHEAD = 3
SMALL = pltpu.CompilerParams(vmem_limit_bytes=16 << 20)


def project_body(x_hbm, w_hbm, gain_hbm, out_ref, x_buf, w_buf, gain_buf, scr, sems):
    pieces = sems.shape[0] - 2
    rows = x_buf.shape[0] // pieces
    weights = pltpu.make_async_copy(w_hbm, w_buf, sems.at[pieces])
    gains = pltpu.make_async_copy(gain_hbm, gain_buf, sems.at[pieces + 1])
    weights.start()
    gains.start()
    copies = []
    for j in range(pieces):
        span = pl.ds(rows * j, rows)
        copies.append(pltpu.make_async_copy(x_hbm.at[span], x_buf.at[span], sems.at[j]))
    for j in range(AHEAD):
        copies[j].start()
    weights.wait()
    gains.wait()
    weight = (w_buf[...].astype(jnp.float32) * gain_buf[...]).T.astype(jnp.bfloat16)
    half = weight.shape[1] // 2
    blocks = x_buf.shape[0] // BLOCK


    def finish(j, part, square):
        turned = (part * lax.rsqrt(square + NORM_EPS)).T
        for b in range(rows // BLOCK):
            for c in range(2):
                place = rows // BLOCK * j + b + blocks * c
                scr[:, place, :] = turned[half * c : half * c + half, BLOCK * b : BLOCK * b + BLOCK]

    waiting = None
    for j in range(pieces):
        copies[j].wait()
        if j + AHEAD < pieces:
            copies[j + AHEAD].start()
        x = x_buf[rows * j : rows * j + rows, :]
        wide = x.astype(jnp.float32)
        square = jnp.mean(wide * wide, axis=1, keepdims=True)
        part = jnp.dot(x, weight, preferred_element_type=jnp.float32)
        if waiting is not None:
            finish(*waiting)
        waiting = (j, part, square)
    finish(*waiting)
    out_ref[...] = scr[...].astype(jnp.bfloat16)


def project(tokens, w_in, gain):
    rows, width = tokens.shape
    channels = w_in.shape[1]
    pieces = 4
    shape = (channels // 2, 2 * rows // BLOCK, BLOCK)
    inputs = [
        pltpu.with_memory_space_constraint(a, pltpu.HBM) for a in (tokens, w_in.T, gain[None])
    ]
    return pl.pallas_call(
        project_body,
        in_specs=[pl.BlockSpec(memory_space=pltpu.HBM)] * 3,
        out_specs=pl.BlockSpec(memory_space=pltpu.VMEM),
        out_shape=pltpu.VMEM(shape, jnp.bfloat16),
        scratch_shapes=[
            pltpu.VMEM((rows, width), jnp.bfloat16),
            pltpu.VMEM((channels, width), jnp.bfloat16),
            pltpu.VMEM((1, width), jnp.float32),
            pltpu.VMEM(shape, jnp.float32),
            pltpu.SemaphoreType.DMA((pieces + 2,)),
        ],
        compiler_params=pltpu.CompilerParams(vmem_limit_bytes=24 << 20),
    )(*inputs)


def fft_tables(total, n_first, n_second):
    scale = 1.0 / math.sqrt(total * GROUP)
    one = np.arange(n_first)
    two = np.arange(n_second)
    first = 2.0 * np.pi * (np.outer(one, one) % n_first) / n_first
    table_one = np.concatenate([np.cos(first), np.sin(first)], 0)
    turn = 2.0 * np.pi * np.outer(one, two) / total
    turns = np.stack([np.cos(turn), np.sin(turn)]) * scale
    second = 2.0 * np.pi * (np.outer(two, two) % n_second) / n_second
    cosine, sine = np.cos(second), np.sin(second)
    table_two = np.block([[cosine, sine], [-sine, cosine]])
    return (
        jnp.asarray(table_one, jnp.bfloat16),
        jnp.asarray(turns, jnp.float32),
        jnp.asarray(table_two, jnp.bfloat16),
    )


def positions_body(x_ref, one_ref, turn_ref, two_ref, out_ref, scr):
    wide = x_ref[...].astype(jnp.float32)
    n_first = wide.shape[0] * 8
    both = [
        wide[:, 8 * c : 8 * c + 8, :].reshape(n_first, BLOCK).astype(jnp.bfloat16)
        for c in range(2)
    ]
    cosine, sine = turn_ref[0], turn_ref[1]
    for c in range(2):
        y = jnp.dot(one_ref[...], both[c], preferred_element_type=jnp.float32)
        y_cos, y_sin = y[:n_first], y[n_first:]
        turned = jnp.concatenate(
            [y_cos * cosine - y_sin * sine, -(y_sin * cosine) - y_cos * sine], 1
        ).astype(jnp.bfloat16)
        z = lax.dot_general(
            two_ref[...], turned, (((1,), (1,)), ((), ())), preferred_element_type=jnp.float32
        )
        for part in range(2):
            for high in range(2):
                scr[:, 4 * c + 2 * part + high, :] = z[
                    BLOCK * part : BLOCK * part + BLOCK, BLOCK * high : BLOCK * high + BLOCK
                ]
    out_ref[...] = scr[...].astype(jnp.bfloat16)


def positions(arrived, total):
    rows = arrived.shape[0]
    tables = fft_tables(total, rows * 8, BLOCK)
    shape = (BLOCK, 8, BLOCK)
    return pl.pallas_call(
        positions_body,
        out_shape=pltpu.VMEM(shape, jnp.bfloat16),
        scratch_shapes=[pltpu.VMEM(shape, jnp.float32)],
        compiler_params=SMALL,
    )(arrived, *tables)


def channel_table(rows):
    source = np.arange(4 * rows)
    core, row, half = source // (2 * rows), source // 2 % rows, source % 2
    place = 2 * half + core
    channel = np.stack([GROUP // 4 * place + row + rows * c for c in range(2)])
    freq = np.arange(GROUP)
    phase = 2.0 * np.pi * (freq[:, None, None] * channel[None] % GROUP) / GROUP
    both = np.stack([np.cos(phase), np.sin(phase)], 2)
    return jnp.asarray(both.reshape(GROUP, -1), jnp.bfloat16)


def channels_body(core_ref, x_ref, table_ref, out_ref, scr):
    core = core_ref[0]
    for k in range(2):
        part = x_ref[k, :, pl.ds(core, 1)]
        count = part.shape[0]
        scr[count * k : count * k + count] = part.reshape(count, *scr.shape[1:]).astype(jnp.float32)
    rows = [
        jnp.concatenate([scr[:, 2 * j, :], scr[:, 2 * j + 1, :]], 1).astype(jnp.bfloat16)
        for j in range(4)
    ]
    data = jnp.concatenate(rows, 0)
    spectrum = jnp.dot(table_ref[...], data, preferred_element_type=jnp.float32)
    out_ref[...] = spectrum.T.astype(jnp.bfloat16)


def channel_mix(core, arrived, table):
    sources, height, width = arrived.shape[1], *arrived.shape[3:]
    return pl.pallas_call(
        channels_body,
        in_specs=[
            pl.BlockSpec(memory_space=pltpu.SMEM),
            pl.BlockSpec(memory_space=pltpu.VMEM),
            pl.BlockSpec(memory_space=pltpu.VMEM),
        ],
        out_shape=pltpu.VMEM((height * width // 4, GROUP), jnp.bfloat16),
        scratch_shapes=[pltpu.VMEM((2 * sources, height, width), jnp.float32)],
        compiler_params=SMALL,
    )(core, arrived, table)


def output_body(chip_ref, spec_ref, *refs):
    *weights, out_ref = refs
    groups = spec_ref.shape[0]
    for flip, ref in enumerate(weights):
        total = None
        for g in range(groups):
            part = jnp.dot(
                spec_ref[g],
                ref[GROUP * g : GROUP * g + GROUP, :],
                preferred_element_type=jnp.float32,
            )
            total = part if total is None else total + part
        out_ref[pl.ds(chip_ref[0] ^ flip, 1)] = total.astype(jnp.bfloat16)[None]


def output_map(chip, gathered, *weights):
    count = gathered.shape[1]
    whole = pl.BlockSpec(memory_space=pltpu.VMEM)
    return pl.pallas_call(
        output_body,
        in_specs=[pl.BlockSpec(memory_space=pltpu.SMEM)] + [whole] * (1 + len(weights)),
        out_shape=pltpu.VMEM((len(weights), count, weights[0].shape[1]), jnp.bfloat16),
        compiler_params=SMALL,
    )(chip, gathered, *weights)


def local(tokens, norm_gain, w_in, w_out):
    rows = lax.axis_size("row")
    total = tokens.shape[0] * rows

    def fetched(flip):
        return lax.ppermute(w_out, ("h", "k"), [(i, i ^ flip) for i in range(4)])

    chip, cross = fetched(2), fetched(3)
    beside = fetched(1)
    projected = project(tokens, w_in, norm_gain)
    arrived = lax.all_to_all(projected, "row", 0, 0, tiled=True)
    core = lax.axis_index("k").astype(jnp.int32).reshape(1)
    place = lax.axis_index(("h", "k")).astype(jnp.int32).reshape(1)
    arrived, core, place = lax.optimization_barrier((arrived, core, place))
    spectra = positions(arrived, total)
    arrived = lax.all_to_all(spectra, ("row", "h"), 0, 0, tiled=True)
    arrived = lax.all_gather(arrived.reshape(2 * rows, 2, *arrived.shape[1:]), "k", axis=0)
    mixed = channel_mix(core, arrived, channel_table(rows))
    gathered = lax.all_gather(mixed, "g", axis=0)
    output = output_map(place, gathered, w_out, beside, chip, cross)
    output = lax.all_to_all(output, ("h", "k"), 0, 0, tiled=True)
    return output.reshape(tokens.shape[0], w_out.shape[1])


def solution(mesh):
    mesh = Mesh(mesh.devices.reshape(32, 4, 2, 2), ("row", "g", "h", "k"))
    columns = ("g", "h", "k")
    placed = (P("row", None), P(), P(None, columns), P(None, columns))
    return jax.shard_map(
        local, mesh=mesh, in_specs=placed, out_specs=P("row", columns), check_vma=False
    )
```

profile of v0, /device:TPU:1, one launch (start us, length us, event | category | flops | bytes accessed | tf_op | source)
XLA Modules:
  0.0 79.1 jit_solution(13087505897049670913)
XLA Ops:
  0.0 0.0 copy-start.4
  0.0 0.0 copy-start.2
  0.0 0.0 copy-start.3
  0.0 0.0 copy-start
  0.0 0.0 copy-start.1
  0.0 4.1 %shard_map.82 = bf16[32,16,128]{2,1,0:T(8,128)(2,1)} custom-call(bf16[1024,2048]{1,0:T(8,128)(2,1)} %x_hbm.1, bf16[64,2048]{1,0:T(8,128)(2,1)} %bitcast.10, f32[1,2048]{1,0:T(1,128)} %bitcast.11), custom_call_target="tpu_custom_call" | custom-call | tf_op jit(solution)/shard_map/pallas_call | solution.py:71
  4.1 13.7 %all-to-all-start = ((bf16[32,16,128]{2,1,0:T(8,128)(2,1)}), bf16[32,16,128]{2,1,0:T(8,128)(2,1)S(1)}, u32[]{:S(2)}, u32[]{:S(2)}) async-start(bf16[32,16,128]{2,1,0:T(8,128)(2,1)} %shard_map.82), calls=%async_computation | async-start | bytes 262144 | tf_op jit(solution)/shard_map/all_to_all | solution.py:219
  17.9 9.3 %all-to-all-done.x_ref = bf16[32,16,128]{2,1,0:T(8,128)(2,1)S(1)} async-done(((bf16[32,16,128]{2,1,0:T(8,128)(2,1)}), bf16[32,16,128]{2,1,0:T(8,128)(2,1)S(1)}, u32[]{:S(2)}, u32[]{:S(2)}) %all-to-all-start) | async-done | bytes 131104 | tf_op jit(solution)/shard_map/all_to_all | solution.py:219
  27.2 0.0 copy-done.4
  27.2 0.0 copy-done.2
  27.2 0.0 copy-done.3
  27.2 1.7 %shard_map.83 = bf16[128,8,128]{2,1,0:T(8,128)(2,1)} custom-call(bf16[32,16,128]{2,1,0:T(8,128)(2,1)S(1)} %all-to-all-done.x_ref, bf16[512,256]{1,0:T(8,128)(2,1)S(1)} %copy-done.3, f32[2,256,128]{2,1,0:T(8,128)S(1)} %copy-done.2, bf16[256,256]{1,0:T(8,128)(2,1)S(1)} %copy-done.4), custom_call_target="tpu_custom_call" | custom-call | tf_op jit(solution)/shard_map/pallas_call | solution.py:134
  28.9 5.1 %all-to-all-start.1 = ((bf16[128,8,128]{2,1,0:T(8,128)(2,1)}), bf16[128,8,128]{2,1,0:T(8,128)(2,1)S(1)}, u32[]{:S(2)}, u32[]{:S(2)}) async-start(bf16[128,8,128]{2,1,0:T(8,128)(2,1)} %shard_map.83), calls=%async_computation.1 | async-start | bytes 524288 | tf_op jit(solution)/shard_map/all_to_all | solution.py:224
  34.0 0.0 copy-done.1
  34.0 2.9 %collective-permute-start.1 = (bf16[1024,128]{1,0:T(8,128)(2,1)S(1)}, bf16[1024,128]{1,0:T(8,128)(2,1)S(1)}, u32[]{:S(2)}, u32[]{:S(2)}) collective-permute-start(bf16[1024,128]{1,0:T(8,128)(2,1)S(1)} %copy-done.1), channel_id=1, source_target_pairs={{0,2},{1,3},{2,0},{3,1},{4,6},{5,7},{6,4},{7,5},{8,10},{9,11},{10,... | collective-permute-start | bytes 786440 | tf_op jit(solution)/shard_map/ppermute | solution.py:214
  36.9 4.6 %collective-permute-start = (bf16[1024,128]{1,0:T(8,128)(2,1)S(1)}, bf16[1024,128]{1,0:T(8,128)(2,1)S(1)}, u32[]{:S(2)}, u32[]{:S(2)}) collective-permute-start(bf16[1024,128]{1,0:T(8,128)(2,1)S(1)} %copy-done.1), channel_id=1, source_target_pairs={{0,1},{1,0},{2,3},{3,2},{4,5},{5,4},{6,7},{7,6},{8,9},{9,8},{10,11... | collective-permute-start | bytes 786440 | tf_op jit(solution)/shard_map/ppermute | solution.py:214
  41.5 2.0 %collective-permute-start.2 = (bf16[1024,128]{1,0:T(8,128)(2,1)S(1)}, bf16[1024,128]{1,0:T(8,128)(2,1)S(1)}, u32[]{:S(2)}, u32[]{:S(2)}) collective-permute-start(bf16[1024,128]{1,0:T(8,128)(2,1)S(1)} %copy-done.1), channel_id=1, source_target_pairs={{0,3},{1,2},{2,1},{3,0},{4,7},{5,6},{6,5},{7,4},{8,11},{9,10},{10,... | collective-permute-start | bytes 786440 | tf_op jit(solution)/shard_map/ppermute | solution.py:214
  43.5 0.6 all-to-all-done.1
  44.1 6.0 %all_gather.9.x_ref = bf16[2,64,2,8,128]{4,3,2,1,0:T(8,128)(2,1)S(1)} all-gather(bf16[1,64,2,8,128]{4,3,2,1,0:T(8,128)(2,1)S(1)} %bitcast.8), channel_id=1, replica_groups=mesh['row'=32,'g'=4,'h'=2,'k'=2] {'k'}, dimensions={0}, use_global_device_ids=true | all-gather | bytes 786432 | tf_op jit(solution)/shard_map/all_gather | solution.py:225
  50.1 0.0 copy-done
  50.1 0.6 shard_map.84
  50.6 16.3 %all-gather = bf16[1024,256]{1,0:T(8,128)(2,1)S(1)} all-gather(bf16[256,256]{1,0:T(8,128)(2,1)S(1)} %shard_map.84), channel_id=2, replica_groups=mesh['row'=32,'g'=4,'h'=2,'k'=2] {'g'}, dimensions={0}, use_global_device_ids=true | all-gather | bytes 655360 | tf_op jit(solution)/shard_map/all_gather | solution.py:227
  66.9 0.0 collective-permute-done.1.refs_2_
  66.9 0.0 collective-permute-done.refs_1_
  66.9 0.0 collective-permute-done.2.refs_3_
  66.9 0.7 shard_map.85
  67.6 10.8 %all_to_all.15 = bf16[4,256,128]{2,1,0:T(8,128)(2,1)S(1)} all-to-all(bf16[4,256,128]{2,1,0:T(8,128)(2,1)S(1)} %shard_map.85), channel_id=1, replica_groups=mesh['row'=32,'g'=4,'h'=2,'k'=2] {'h','k'}, dimensions={0} | all-to-all | bytes 524288 | tf_op jit(solution)/shard_map/all_to_all | solution.py:229
  78.4 0.7 copy.10
Async XLA Ops:
  0.0 27.2 %copy-start.4 = (bf16[256,256]{1,0:T(8,128)(2,1)S(1)}, bf16[256,256]{1,0:T(8,128)(2,1)}, u32[]{:S(2)}) copy-start(bf16[256,256]{1,0:T(8,128)(2,1)} %constant.18.clone.two_ref) | copy-start | bytes 393220
  0.0 27.2 %copy-start.2 = (f32[2,256,128]{2,1,0:T(8,128)S(1)}, f32[2,256,128]{2,1,0:T(8,128)}, u32[]{:S(2)}) copy-start(f32[2,256,128]{2,1,0:T(8,128)} %constant.17.clone.turn_ref) | copy-start | bytes 786436
  0.0 27.2 %copy-start.3 = (bf16[512,256]{1,0:T(8,128)(2,1)S(1)}, bf16[512,256]{1,0:T(8,128)(2,1)}, u32[]{:S(2)}) copy-start(bf16[512,256]{1,0:T(8,128)(2,1)} %constant.16.clone.one_ref) | copy-start | bytes 786436
  0.0 50.1 %copy-start = (bf16[256,512]{1,0:T(8,128)(2,1)S(1)}, bf16[256,512]{1,0:T(8,128)(2,1)}, u32[]{:S(2)}) copy-start(bf16[256,512]{1,0:T(8,128)(2,1)} %constant.19.clone.table_ref) | copy-start | bytes 786436
  0.0 34.0 %copy-start.1 = (bf16[1024,128]{1,0:T(8,128)(2,1)S(1)}, bf16[1024,128]{1,0:T(8,128)(2,1)}, u32[]{:S(2)}) copy-start(bf16[1024,128]{1,0:T(8,128)(2,1)} %refs_0_.1) | copy-start | bytes 786436
  4.1 23.1 %all-to-all-start = ((bf16[32,16,128]{2,1,0:T(8,128)(2,1)}), bf16[32,16,128]{2,1,0:T(8,128)(2,1)S(1)}, u32[]{:S(2)}, u32[]{:S(2)}) async-start(bf16[32,16,128]{2,1,0:T(8,128)(2,1)} %shard_map.82), calls=%async_computation | async-start | bytes 262144 | tf_op jit(solution)/shard_map/all_to_all | solution.py:219
  28.9 15.2 %all-to-all-start.1 = ((bf16[128,8,128]{2,1,0:T(8,128)(2,1)}), bf16[128,8,128]{2,1,0:T(8,128)(2,1)S(1)}, u32[]{:S(2)}, u32[]{:S(2)}) async-start(bf16[128,8,128]{2,1,0:T(8,128)(2,1)} %shard_map.83), calls=%async_computation.1 | async-start | bytes 524288 | tf_op jit(solution)/shard_map/all_to_all | solution.py:224
  34.0 32.9 %collective-permute-start.1 = (bf16[1024,128]{1,0:T(8,128)(2,1)S(1)}, bf16[1024,128]{1,0:T(8,128)(2,1)S(1)}, u32[]{:S(2)}, u32[]{:S(2)}) collective-permute-start(bf16[1024,128]{1,0:T(8,128)(2,1)S(1)} %copy-done.1), channel_id=1, source_target_pairs={{0,2},{1,3},{2,0},{3,1},{4,6},{5,7},{6,4},{7,5},{8,10},{9,11},{10,... | collective-permute-start | bytes 786440 | tf_op jit(solution)/shard_map/ppermute | solution.py:214
  36.9 30.0 %collective-permute-start = (bf16[1024,128]{1,0:T(8,128)(2,1)S(1)}, bf16[1024,128]{1,0:T(8,128)(2,1)S(1)}, u32[]{:S(2)}, u32[]{:S(2)}) collective-permute-start(bf16[1024,128]{1,0:T(8,128)(2,1)S(1)} %copy-done.1), channel_id=1, source_target_pairs={{0,1},{1,0},{2,3},{3,2},{4,5},{5,4},{6,7},{7,6},{8,9},{9,8},{10,11... | collective-permute-start | bytes 786440 | tf_op jit(solution)/shard_map/ppermute | solution.py:214
  41.5 25.4 %collective-permute-start.2 = (bf16[1024,128]{1,0:T(8,128)(2,1)S(1)}, bf16[1024,128]{1,0:T(8,128)(2,1)S(1)}, u32[]{:S(2)}, u32[]{:S(2)}) collective-permute-start(bf16[1024,128]{1,0:T(8,128)(2,1)S(1)} %copy-done.1), channel_id=1, source_target_pairs={{0,3},{1,2},{2,1},{3,0},{4,7},{5,6},{6,5},{7,4},{8,11},{9,10},{10,... | collective-permute-start | bytes 786440 | tf_op jit(solution)/shard_map/ppermute | solution.py:214
where the time goes:
time: 79.5 us; the launch traced here: 79.1 us
  blocking collectives  33.1 us (42%)
  starting transfers between devices  28.3 us (36%)
  waiting for transfers between devices  9.92 us (12%)
  Pallas kernels  7.02 us (9%)
    all_gather x1, blocking collectives, local(): gathered = lax.all_gather(mixed, 'g', axis=0)  16.3 us
    all_to_all x1, starting transfers between devices, local(): arrived = lax.all_to_all(projected, 'row', 0, 0, tiled=True)  13.7 us
    all_to_all x1, blocking collectives, local(): output = lax.all_to_all(output, ('h', 'k'), 0, 0, tiled=True)  10.8 us
    ppermute x3, starting transfers between devices, fetched(): return lax.ppermute(w_out, ('h', 'k'), [(i, i ^ flip) for i in range(4)])  9.47 us
    all_to_all x1, waiting for transfers between devices, local(): arrived = lax.all_to_all(projected, 'row', 0, 0, tiled=True)  9.34 us
    all_gather x1, blocking collectives, local(): lax.all_gather(arrived.reshape(2 * rows, 2, *arrived.shape[1:]), 'k', axi...  5.99 us
    all_to_all x1, starting transfers between devices, local(): arrived = lax.all_to_all(spectra, ('row', 'h'), 0, 0, tiled=True)  5.12 us
    pallas_call x1, Pallas kernels, project(): pl.pallas_call(project_body, in_specs=[pl.BlockSpec(memory_space=pltpu.HB...  4.08 us
  transfers between devices with their start and end apart: 5, of which 2 were waited for; matrix products, arithmetic and copies ran while one was open for 0% of the time, Pallas kernels for 1%

commit v1 on v0

--- a/solution.py
+++ b/solution.py
@@ -180,10 +180,10 @@
     )(core, arrived, table)
 
 
-def output_body(chip_ref, spec_ref, *refs):
-    *weights, out_ref = refs
+def output_body(spec_ref, *refs):
+    weights, outs = refs[: len(refs) // 2], refs[len(refs) // 2 :]
     groups = spec_ref.shape[0]
-    for flip, ref in enumerate(weights):
+    for ref, out_ref in zip(weights, outs):
         total = None
         for g in range(groups):
             part = jnp.dot(
@@ -192,42 +192,64 @@
                 preferred_element_type=jnp.float32,
             )
             total = part if total is None else total + part
-        out_ref[pl.ds(chip_ref[0] ^ flip, 1)] = total.astype(jnp.bfloat16)[None]
-
-
-def output_map(chip, gathered, *weights):
-    count = gathered.shape[1]
+        out_ref[...] = total.astype(jnp.bfloat16)
+
+
+def output_map(gathered, *weights):
+    part = pltpu.VMEM((gathered.shape[1], weights[0].shape[1]), jnp.bfloat16)
+    return pl.pallas_call(
+        output_body, out_shape=[part] * len(weights), compiler_params=SMALL
+    )(gathered, *weights)
+
+
+def join_body(place_ref, *refs):
+    *parts, out_ref, sems = refs
+    count = parts[0].shape[0]
+    copies = []
+    for flip, part in enumerate(parts):
+        span = pl.ds(pl.multiple_of((place_ref[0] ^ flip) * count, count), count)
+        copies.append(pltpu.make_async_copy(part, out_ref.at[span], sems.at[flip]))
+        copies[flip].start()
+    for copy in copies:
+        copy.wait()
+
+
+def join(place, *parts):
+    count, width = parts[0].shape
     whole = pl.BlockSpec(memory_space=pltpu.VMEM)
     return pl.pallas_call(
-        output_body,
-        in_specs=[pl.BlockSpec(memory_space=pltpu.SMEM)] + [whole] * (1 + len(weights)),
-        out_shape=pltpu.VMEM((len(weights), count, weights[0].shape[1]), jnp.bfloat16),
+        join_body,
+        in_specs=[pl.BlockSpec(memory_space=pltpu.SMEM)] + [whole] * len(parts),
+        out_specs=pl.BlockSpec(memory_space=pltpu.HBM),
+        out_shape=jax.ShapeDtypeStruct((count * len(parts), width), jnp.bfloat16),
+        scratch_shapes=[pltpu.SemaphoreType.DMA((len(parts),))],
         compiler_params=SMALL,
-    )(chip, gathered, *weights)
+    )(place, *parts)
 
 
 def local(tokens, norm_gain, w_in, w_out):
     rows = lax.axis_size("row")
     total = tokens.shape[0] * rows
 
-    def fetched(flip):
-        return lax.ppermute(w_out, ("h", "k"), [(i, i ^ flip) for i in range(4)])
-
-    chip, cross = fetched(2), fetched(3)
-    beside = fetched(1)
+    def sent(part, flip):
+        return lax.ppermute(part, ("h", "k"), [(i, i ^ flip) for i in range(4)])
+
+    w_chip, w_cross = sent(w_out, 2), sent(w_out, 3)
+    w_core = sent(w_out, 1)
     projected = project(tokens, w_in, norm_gain)
     arrived = lax.all_to_all(projected, "row", 0, 0, tiled=True)
-    core = lax.axis_index("k").astype(jnp.int32).reshape(1)
-    place = lax.axis_index(("h", "k")).astype(jnp.int32).reshape(1)
-    arrived, core, place = lax.optimization_barrier((arrived, core, place))
     spectra = positions(arrived, total)
     arrived = lax.all_to_all(spectra, ("row", "h"), 0, 0, tiled=True)
     arrived = lax.all_gather(arrived.reshape(2 * rows, 2, *arrived.shape[1:]), "k", axis=0)
+    core = lax.axis_index("k").astype(jnp.int32).reshape(1)
     mixed = channel_mix(core, arrived, channel_table(rows))
     gathered = lax.all_gather(mixed, "g", axis=0)
-    output = output_map(place, gathered, w_out, beside, chip, cross)
-    output = lax.all_to_all(output, ("h", "k"), 0, 0, tiled=True)
-    return output.reshape(tokens.shape[0], w_out.shape[1])
+    chip, cross = output_map(gathered, w_chip, w_cross)
+    chip, cross = sent(chip, 2), sent(cross, 3)
+    mine, near = output_map(gathered, w_out, w_core)
+    near = sent(near, 1)
+    place = lax.axis_index(("h", "k")).astype(jnp.int32).reshape(1)
+    return join(place, mine, near, chip, cross)
 
 
 def solution(mesh):

time: 79.5 us -> 79.9 us (level)
  blocking collectives: 33.1 us -> 45.1 us
  waiting for transfers between devices: 9.92 us -> 1.79 us
  starting transfers between devices: 28.3 us -> 25.2 us
    all_to_all x1 -> x0, starting transfers between devices: 13.7 us -> none  [local(): arrived = lax.all_to_all(projected, 'row', 0, 0, tiled=True)]
    all_to_all x1, blocking collectives: 10.8 us -> 22.8 us  [local(): arrived = lax.all_to_all(projected, 'row', 0, 0, tiled=True)]
    ppermute x3 -> x6, starting transfers between devices: 9.47 us -> 20.1 us  [sent(): return lax.ppermute(part, ('h', 'k'), [(i, i ^ flip) for i in range(4)])]
    all_to_all x1 -> x0, waiting for transfers between devices: 9.34 us -> none  [local(): arrived = lax.all_to_all(projected, 'row', 0, 0, tiled=True)]
    ppermute x3 -> x6, waiting for transfers between devices: 0.01 us -> 1.21 us  [sent(): return lax.ppermute(part, ('h', 'k'), [(i, i ^ flip) for i in range(4)])]
    pallas_call x1 -> x3, Pallas kernels: 0.71 us -> 1.57 us  [the longest x2 0.85 us: output_map(): pl.pallas_call(output_body, out_shape=[part] * len(weights), compiler_par...]
  transfers between devices with their start and end apart: 5 -> 7, of which waited for: 2 -> 2; matrix products, arithmetic and copies ran while one was open for 0% -> 0% of each run, Pallas kernels for 1% -> 2%
where the time goes in v1:
time: 79.9 us; the launch traced here: 79.5 us
  blocking collectives  45.1 us (56%)
  starting transfers between devices  25.2 us (32%)
  Pallas kernels  7.22 us (9%)
  waiting for transfers between devices  1.79 us (2%)
    all_to_all x1, blocking collectives, local(): arrived = lax.all_to_all(projected, 'row', 0, 0, tiled=True)  22.8 us
    ppermute x6, starting transfers between devices, sent(): return lax.ppermute(part, ('h', 'k'), [(i, i ^ flip) for i in range(4)])  20.1 us
    all_gather x1, blocking collectives, local(): gathered = lax.all_gather(mixed, 'g', axis=0)  16.3 us
    all_gather x1, blocking collectives, local(): lax.all_gather(arrived.reshape(2 * rows, 2, *arrived.shape[1:]), 'k', axi...  5.97 us
    all_to_all x1, starting transfers between devices, local(): arrived = lax.all_to_all(spectra, ('row', 'h'), 0, 0, tiled=True)  5.13 us
    pallas_call x1, Pallas kernels, project(): pl.pallas_call(project_body, in_specs=[pl.BlockSpec(memory_space=pltpu.HB...  3.42 us
    pallas_call x1, Pallas kernels, positions(): pl.pallas_call(positions_body, out_shape=pltpu.VMEM(shape, jnp.bfloat16),...  1.67 us
  transfers between devices with their start and end apart: 7, of which 2 were waited for; matrix products, arithmetic and copies ran while one was open for 0% of the time, Pallas kernels for 2%

profile of v1, /device:TPU:1, one launch (start us, length us, event | category | flops | bytes accessed | tf_op | source)
XLA Modules:
  0.0 79.5 jit_solution(3402694701772935877)
XLA Ops:
  0.0 0.0 copy-start.3
  0.0 0.0 copy-start.4
  0.0 0.0 copy-start
  0.0 0.0 copy-start.1
  0.0 3.4 %shard_map.82 = bf16[32,16,128]{2,1,0:T(8,128)(2,1)S(1)} custom-call(bf16[1024,2048]{1,0:T(8,128)(2,1)} %x_hbm.1, bf16[64,2048]{1,0:T(8,128)(2,1)} %bitcast.9, f32[1,2048]{1,0:T(1,128)} %bitcast.10), custom_call_target="tpu_custom_call" | custom-call | tf_op jit(solution)/shard_map/pallas_call | solution.py:71
  3.5 22.8 %all_to_all.10.x_ref = bf16[32,16,128]{2,1,0:T(8,128)(2,1)S(1)} all-to-all(bf16[32,16,128]{2,1,0:T(8,128)(2,1)S(1)} %shard_map.82), channel_id=1, replica_groups=mesh['row'=32,'g'=4,'h'=2,'k'=2] {'row'}, dimensions={0} | all-to-all | bytes 262144 | tf_op jit(solution)/shard_map/all_to_all | solution.py:240
  26.3 0.0 copy-done.2
  26.3 0.0 copy-done.3
  26.3 0.0 copy-done.4
  26.3 1.7 %shard_map.83 = bf16[128,8,128]{2,1,0:T(8,128)(2,1)} custom-call(bf16[32,16,128]{2,1,0:T(8,128)(2,1)S(1)} %all_to_all.10.x_ref, bf16[512,256]{1,0:T(8,128)(2,1)S(1)} %copy-done.2, f32[2,256,128]{2,1,0:T(8,128)S(1)} %copy-done.3, bf16[256,256]{1,0:T(8,128)(2,1)S(1)} %copy-done.4), custom_call_target="tpu_custom_call" | custom-call | tf_op jit(solution)/shard_map/pallas_call | solution.py:134
  28.0 5.1 %all-to-all-start.1 = ((bf16[128,8,128]{2,1,0:T(8,128)(2,1)}), bf16[128,8,128]{2,1,0:T(8,128)(2,1)S(1)}, u32[]{:S(2)}, u32[]{:S(2)}) async-start(bf16[128,8,128]{2,1,0:T(8,128)(2,1)} %shard_map.83), calls=%async_computation.1 | async-start | bytes 524288 | tf_op jit(solution)/shard_map/all_to_all | solution.py:242
  33.1 0.0 copy-done.1
  33.1 2.9 %collective-permute-start.2 = (bf16[1024,128]{1,0:T(8,128)(2,1)S(1)}, bf16[1024,128]{1,0:T(8,128)(2,1)S(1)}, u32[]{:S(2)}, u32[]{:S(2)}) collective-permute-start(bf16[1024,128]{1,0:T(8,128)(2,1)S(1)} %copy-done.1), channel_id=1, source_target_pairs={{0,2},{1,3},{2,0},{3,1},{4,6},{5,7},{6,4},{7,5},{8,10},{9,11},{10,... | collective-permute-start | bytes 786440 | tf_op jit(solution)/shard_map/ppermute | solution.py:235
  36.1 4.6 %collective-permute-start.3 = (bf16[1024,128]{1,0:T(8,128)(2,1)S(1)}, bf16[1024,128]{1,0:T(8,128)(2,1)S(1)}, u32[]{:S(2)}, u32[]{:S(2)}) collective-permute-start(bf16[1024,128]{1,0:T(8,128)(2,1)S(1)} %copy-done.1), channel_id=1, source_target_pairs={{0,3},{1,2},{2,1},{3,0},{4,7},{5,6},{6,5},{7,4},{8,11},{9,10},{10,... | collective-permute-start | bytes 786440 | tf_op jit(solution)/shard_map/ppermute | solution.py:235
  40.7 1.9 %collective-permute-start = (bf16[1024,128]{1,0:T(8,128)(2,1)S(1)}, bf16[1024,128]{1,0:T(8,128)(2,1)S(1)}, u32[]{:S(2)}, u32[]{:S(2)}) collective-permute-start(bf16[1024,128]{1,0:T(8,128)(2,1)S(1)} %copy-done.1), channel_id=1, source_target_pairs={{0,1},{1,0},{2,3},{3,2},{4,5},{5,4},{6,7},{7,6},{8,9},{9,8},{10,11... | collective-permute-start | bytes 786440 | tf_op jit(solution)/shard_map/ppermute | solution.py:235
  42.6 0.6 all-to-all-done.1
  43.2 6.0 %all_gather.9.x_ref = bf16[2,64,2,8,128]{4,3,2,1,0:T(8,128)(2,1)S(1)} all-gather(bf16[1,64,2,8,128]{4,3,2,1,0:T(8,128)(2,1)S(1)} %bitcast.8), channel_id=1, replica_groups=mesh['row'=32,'g'=4,'h'=2,'k'=2] {'k'}, dimensions={0}, use_global_device_ids=true | all-gather | bytes 786432 | tf_op jit(solution)/shard_map/all_gather | solution.py:243
  49.2 0.0 copy-done
  49.2 0.6 shard_map.84
  49.7 16.3 %all-gather = bf16[1024,256]{1,0:T(8,128)(2,1)S(1)} all-gather(bf16[256,256]{1,0:T(8,128)(2,1)S(1)} %shard_map.84), channel_id=2, replica_groups=mesh['row'=32,'g'=4,'h'=2,'k'=2] {'g'}, dimensions={0}, use_global_device_ids=true | all-gather | bytes 655360 | tf_op jit(solution)/shard_map/all_gather | solution.py:246
  66.0 0.0 collective-permute-done.2.refs_0_
  66.0 0.0 collective-permute-done.3.refs_1_
  66.0 0.4 shard_map.86
  66.5 3.3 %collective-permute-start.4 = (bf16[256,128]{1,0:T(8,128)(2,1)S(1)}, bf16[256,128]{1,0:T(8,128)(2,1)S(1)}, u32[]{:S(2)}, u32[]{:S(2)}) collective-permute-start(bf16[256,128]{1,0:T(8,128)(2,1)S(1)} %get-tuple-element.11), channel_id=1, source_target_pairs={{0,2},{1,3},{2,0},{3,1},{4,6},{5,7},{6,4},{7,5},{8,10},{9,11},{10,... | collective-permute-start | bytes 196616 | tf_op jit(solution)/shard_map/ppermute | solution.py:235
  69.8 5.4 %collective-permute-start.5 = (bf16[256,128]{1,0:T(8,128)(2,1)S(1)}, bf16[256,128]{1,0:T(8,128)(2,1)S(1)}, u32[]{:S(2)}, u32[]{:S(2)}) collective-permute-start(bf16[256,128]{1,0:T(8,128)(2,1)S(1)} %get-tuple-element.12), channel_id=1, source_target_pairs={{0,3},{1,2},{2,1},{3,0},{4,7},{5,6},{6,5},{7,4},{8,11},{9,10},{10,... | collective-permute-start | bytes 196616 | tf_op jit(solution)/shard_map/ppermute | solution.py:235
  75.2 0.0 collective-permute-done.refs_1_
  75.2 0.4 shard_map.85
  75.6 1.9 %collective-permute-start.1 = (bf16[256,128]{1,0:T(8,128)(2,1)S(1)}, bf16[256,128]{1,0:T(8,128)(2,1)S(1)}, u32[]{:S(2)}, u32[]{:S(2)}) collective-permute-start(bf16[256,128]{1,0:T(8,128)(2,1)S(1)} %get-tuple-element.10), channel_id=1, source_target_pairs={{0,1},{1,0},{2,3},{3,2},{4,5},{5,4},{6,7},{7,6},{8,9},{9,8},{10,11... | collective-permute-start | bytes 196616 | tf_op jit(solution)/shard_map/ppermute | solution.py:235
  77.6 0.0 collective-permute-done.4.refs_2_
  77.6 0.0 collective-permute-done.5.refs_3_
  77.6 1.2 %collective-permute-done.1.refs_1_ = bf16[256,128]{1,0:T(8,128)(2,1)S(1)} collective-permute-done((bf16[256,128]{1,0:T(8,128)(2,1)S(1)}, bf16[256,128]{1,0:T(8,128)(2,1)S(1)}, u32[]{:S(2)}, u32[]{:S(2)}) %collective-permute-start.1) | collective-permute-done | bytes 65568 | tf_op jit(solution)/shard_map/ppermute | solution.py:235
  78.8 0.7 shard_map.87
  (1 shorter events, 0.0 us)
Async XLA Ops:
  0.0 26.3 %copy-start.2 = (bf16[512,256]{1,0:T(8,128)(2,1)S(1)}, bf16[512,256]{1,0:T(8,128)(2,1)}, u32[]{:S(2)}) copy-start(bf16[512,256]{1,0:T(8,128)(2,1)} %constant.16.clone.one_ref) | copy-start | bytes 786436
  0.0 26.3 %copy-start.3 = (f32[2,256,128]{2,1,0:T(8,128)S(1)}, f32[2,256,128]{2,1,0:T(8,128)}, u32[]{:S(2)}) copy-start(f32[2,256,128]{2,1,0:T(8,128)} %constant.17.clone.turn_ref) | copy-start | bytes 786436
  0.0 26.3 %copy-start.4 = (bf16[256,256]{1,0:T(8,128)(2,1)S(1)}, bf16[256,256]{1,0:T(8,128)(2,1)}, u32[]{:S(2)}) copy-start(bf16[256,256]{1,0:T(8,128)(2,1)} %constant.18.clone.two_ref) | copy-start | bytes 393220
  0.0 49.2 %copy-start = (bf16[256,512]{1,0:T(8,128)(2,1)S(1)}, bf16[256,512]{1,0:T(8,128)(2,1)}, u32[]{:S(2)}) copy-start(bf16[256,512]{1,0:T(8,128)(2,1)} %constant.19.clone.table_ref) | copy-start | bytes 786436
  0.0 33.1 %copy-start.1 = (bf16[1024,128]{1,0:T(8,128)(2,1)S(1)}, bf16[1024,128]{1,0:T(8,128)(2,1)}, u32[]{:S(2)}) copy-start(bf16[1024,128]{1,0:T(8,128)(2,1)} %refs_0_.1) | copy-start | bytes 786436
  28.0 15.2 %all-to-all-start.1 = ((bf16[128,8,128]{2,1,0:T(8,128)(2,1)}), bf16[128,8,128]{2,1,0:T(8,128)(2,1)S(1)}, u32[]{:S(2)}, u32[]{:S(2)}) async-start(bf16[128,8,128]{2,1,0:T(8,128)(2,1)} %shard_map.83), calls=%async_computation.1 | async-start | bytes 524288 | tf_op jit(solution)/shard_map/all_to_all | solution.py:242
  33.1 32.9 %collective-permute-start.2 = (bf16[1024,128]{1,0:T(8,128)(2,1)S(1)}, bf16[1024,128]{1,0:T(8,128)(2,1)S(1)}, u32[]{:S(2)}, u32[]{:S(2)}) collective-permute-start(bf16[1024,128]{1,0:T(8,128)(2,1)S(1)} %copy-done.1), channel_id=1, source_target_pairs={{0,2},{1,3},{2,0},{3,1},{4,6},{5,7},{6,4},{7,5},{8,10},{9,11},{10,... | collective-permute-start | bytes 786440 | tf_op jit(solution)/shard_map/ppermute | solution.py:235
  36.1 30.0 %collective-permute-start.3 = (bf16[1024,128]{1,0:T(8,128)(2,1)S(1)}, bf16[1024,128]{1,0:T(8,128)(2,1)S(1)}, u32[]{:S(2)}, u32[]{:S(2)}) collective-permute-start(bf16[1024,128]{1,0:T(8,128)(2,1)S(1)} %copy-done.1), channel_id=1, source_target_pairs={{0,3},{1,2},{2,1},{3,0},{4,7},{5,6},{6,5},{7,4},{8,11},{9,10},{10,... | collective-permute-start | bytes 786440 | tf_op jit(solution)/shard_map/ppermute | solution.py:235
  40.7 34.5 %collective-permute-start = (bf16[1024,128]{1,0:T(8,128)(2,1)S(1)}, bf16[1024,128]{1,0:T(8,128)(2,1)S(1)}, u32[]{:S(2)}, u32[]{:S(2)}) collective-permute-start(bf16[1024,128]{1,0:T(8,128)(2,1)S(1)} %copy-done.1), channel_id=1, source_target_pairs={{0,1},{1,0},{2,3},{3,2},{4,5},{5,4},{6,7},{7,6},{8,9},{9,8},{10,11... | collective-permute-start | bytes 786440 | tf_op jit(solution)/shard_map/ppermute | solution.py:235
  66.5 11.1 %collective-permute-start.4 = (bf16[256,128]{1,0:T(8,128)(2,1)S(1)}, bf16[256,128]{1,0:T(8,128)(2,1)S(1)}, u32[]{:S(2)}, u32[]{:S(2)}) collective-permute-start(bf16[256,128]{1,0:T(8,128)(2,1)S(1)} %get-tuple-element.11), channel_id=1, source_target_pairs={{0,2},{1,3},{2,0},{3,1},{4,6},{5,7},{6,4},{7,5},{8,10},{9,11},{10,... | collective-permute-start | bytes 196616 | tf_op jit(solution)/shard_map/ppermute | solution.py:235
  69.8 7.8 %collective-permute-start.5 = (bf16[256,128]{1,0:T(8,128)(2,1)S(1)}, bf16[256,128]{1,0:T(8,128)(2,1)S(1)}, u32[]{:S(2)}, u32[]{:S(2)}) collective-permute-start(bf16[256,128]{1,0:T(8,128)(2,1)S(1)} %get-tuple-element.12), channel_id=1, source_target_pairs={{0,3},{1,2},{2,1},{3,0},{4,7},{5,6},{6,5},{7,4},{8,11},{9,10},{10,... | collective-permute-start | bytes 196616 | tf_op jit(solution)/shard_map/ppermute | solution.py:235
  75.6 3.1 %collective-permute-start.1 = (bf16[256,128]{1,0:T(8,128)(2,1)S(1)}, bf16[256,128]{1,0:T(8,128)(2,1)S(1)}, u32[]{:S(2)}, u32[]{:S(2)}) collective-permute-start(bf16[256,128]{1,0:T(8,128)(2,1)S(1)} %get-tuple-element.10), channel_id=1, source_target_pairs={{0,1},{1,0},{2,3},{3,2},{4,5},{5,4},{6,7},{7,6},{8,9},{9,8},{10,11... | collective-permute-start | bytes 196616 | tf_op jit(solution)/shard_map/ppermute | solution.py:235

commit v2 on v0

--- a/solution.py
+++ b/solution.py
@@ -210,21 +210,21 @@
     rows = lax.axis_size("row")
     total = tokens.shape[0] * rows
 
-    def fetched(flip):
-        return lax.ppermute(w_out, ("h", "k"), [(i, i ^ flip) for i in range(4)])
-
-    chip, cross = fetched(2), fetched(3)
-    beside = fetched(1)
+    def sent(part, flip):
+        return lax.ppermute(part, ("h", "k"), [(i, i ^ flip) for i in range(4)])
+
+    chip = sent(w_out, 2)
+    beside = sent(w_out, 1)
+    cross = sent(beside, 2)
     projected = project(tokens, w_in, norm_gain)
     arrived = lax.all_to_all(projected, "row", 0, 0, tiled=True)
-    core = lax.axis_index("k").astype(jnp.int32).reshape(1)
-    place = lax.axis_index(("h", "k")).astype(jnp.int32).reshape(1)
-    arrived, core, place = lax.optimization_barrier((arrived, core, place))
     spectra = positions(arrived, total)
     arrived = lax.all_to_all(spectra, ("row", "h"), 0, 0, tiled=True)
     arrived = lax.all_gather(arrived.reshape(2 * rows, 2, *arrived.shape[1:]), "k", axis=0)
+    core = lax.axis_index("k").astype(jnp.int32).reshape(1)
     mixed = channel_mix(core, arrived, channel_table(rows))
     gathered = lax.all_gather(mixed, "g", axis=0)
+    place = lax.axis_index(("h", "k")).astype(jnp.int32).reshape(1)
     output = output_map(place, gathered, w_out, beside, chip, cross)
     output = lax.all_to_all(output, ("h", "k"), 0, 0, tiled=True)
     return output.reshape(tokens.shape[0], w_out.shape[1])

time: 79.5 us -> 78 us (0.981)
  blocking collectives: 33.1 us -> 55.2 us
  starting transfers between devices: 28.3 us -> 14.4 us
  waiting for transfers between devices: 9.92 us -> 0.82 us
    all_to_all x0 -> x1, blocking collectives: none -> 22.9 us  [local(): arrived = lax.all_to_all(projected, 'row', 0, 0, tiled=True)]
    all_to_all x1 -> x0, starting transfers between devices: 13.7 us -> none  [local(): arrived = lax.all_to_all(projected, 'row', 0, 0, tiled=True)]
    all_to_all x1 -> x0, waiting for transfers between devices: 9.34 us -> none  [local(): arrived = lax.all_to_all(projected, 'row', 0, 0, tiled=True)]
    all_gather x1, blocking collectives: 16.3 us -> 15.1 us  [local(): gathered = lax.all_gather(mixed, 'g', axis=0)]
  transfers between devices with their start and end apart: 5 -> 4, of which waited for: 2 -> 1; matrix products, arithmetic and copies ran while one was open for 0% -> 0% of each run, Pallas kernels for 1% -> 1%
where the time goes in v2:
time: 78 us; the launch traced here: 77.7 us
  blocking collectives  55.2 us (71%)
  starting transfers between devices  14.4 us (18%)
  Pallas kernels  6.36 us (8%)
  waiting for transfers between devices  0.82 us (1%)
    all_to_all x1, blocking collectives, local(): arrived = lax.all_to_all(projected, 'row', 0, 0, tiled=True)  22.9 us
    all_gather x1, blocking collectives, local(): gathered = lax.all_gather(mixed, 'g', axis=0)  15.1 us
    all_to_all x1, blocking collectives, local(): output = lax.all_to_all(output, ('h', 'k'), 0, 0, tiled=True)  11.6 us
    ppermute x3, starting transfers between devices, sent(): return lax.ppermute(part, ('h', 'k'), [(i, i ^ flip) for i in range(4)])  9.29 us
    all_gather x1, blocking collectives, local(): lax.all_gather(arrived.reshape(2 * rows, 2, *arrived.shape[1:]), 'k', axi...  5.75 us
    all_to_all x1, starting transfers between devices, local(): arrived = lax.all_to_all(spectra, ('row', 'h'), 0, 0, tiled=True)  5.12 us
    pallas_call x1, Pallas kernels, project(): pl.pallas_call(project_body, in_specs=[pl.BlockSpec(memory_space=pltpu.HB...  3.42 us
    pallas_call x1, Pallas kernels, positions(): pl.pallas_call(positions_body, out_shape=pltpu.VMEM(shape, jnp.bfloat16),...  1.67 us
  transfers between devices with their start and end apart: 4, of which 1 were waited for; matrix products, arithmetic and copies ran while one was open for 0% of the time, Pallas kernels for 1%

profile of v2, /device:TPU:1, one launch (start us, length us, event | category | flops | bytes accessed | tf_op | source)
XLA Modules:
  0.0 77.7 jit_solution(8085524177464969318)
XLA Ops:
  0.0 0.0 copy-start.4
  0.0 0.0 copy-start.2
  0.0 0.0 copy-start.3
  0.0 0.0 copy-start
  0.0 0.0 copy-start.1
  0.0 3.4 %shard_map.82 = bf16[32,16,128]{2,1,0:T(8,128)(2,1)S(1)} custom-call(bf16[1024,2048]{1,0:T(8,128)(2,1)} %x_hbm.1, bf16[64,2048]{1,0:T(8,128)(2,1)} %bitcast.10, f32[1,2048]{1,0:T(1,128)} %bitcast.11), custom_call_target="tpu_custom_call" | custom-call | tf_op jit(solution)/shard_map/pallas_call | solution.py:71
  3.5 22.9 %all_to_all.15.x_ref = bf16[32,16,128]{2,1,0:T(8,128)(2,1)S(1)} all-to-all(bf16[32,16,128]{2,1,0:T(8,128)(2,1)S(1)} %shard_map.82), channel_id=1, replica_groups=mesh['row'=32,'g'=4,'h'=2,'k'=2] {'row'}, dimensions={0} | all-to-all | bytes 262144 | tf_op jit(solution)/shard_map/all_to_all | solution.py:220
  26.3 0.0 copy-done.4
  26.3 0.0 copy-done.2
  26.3 0.0 copy-done.3
  26.3 1.7 %shard_map.83 = bf16[128,8,128]{2,1,0:T(8,128)(2,1)} custom-call(bf16[32,16,128]{2,1,0:T(8,128)(2,1)S(1)} %all_to_all.15.x_ref, bf16[512,256]{1,0:T(8,128)(2,1)S(1)} %copy-done.3, f32[2,256,128]{2,1,0:T(8,128)S(1)} %copy-done.2, bf16[256,256]{1,0:T(8,128)(2,1)S(1)} %copy-done.4), custom_call_target="tpu_custom_call" | custom-call | tf_op jit(solution)/shard_map/pallas_call | solution.py:134
  28.0 5.1 %all-to-all-start.1 = ((bf16[128,8,128]{2,1,0:T(8,128)(2,1)}), bf16[128,8,128]{2,1,0:T(8,128)(2,1)S(1)}, u32[]{:S(2)}, u32[]{:S(2)}) async-start(bf16[128,8,128]{2,1,0:T(8,128)(2,1)} %shard_map.83), calls=%async_computation.1 | async-start | bytes 524288 | tf_op jit(solution)/shard_map/all_to_all | solution.py:222
  33.1 0.0 copy-done.1
  33.1 4.0 %collective-permute-start = (bf16[1024,128]{1,0:T(8,128)(2,1)S(1)}, bf16[1024,128]{1,0:T(8,128)(2,1)S(1)}, u32[]{:S(2)}, u32[]{:S(2)}) collective-permute-start(bf16[1024,128]{1,0:T(8,128)(2,1)S(1)} %copy-done.1), channel_id=1, source_target_pairs={{0,1},{1,0},{2,3},{3,2},{4,5},{5,4},{6,7},{7,6},{8,9},{9,8},{10,11... | collective-permute-start | bytes 786440 | tf_op jit(solution)/shard_map/ppermute | solution.py:214
  37.1 3.2 %collective-permute-start.1 = (bf16[1024,128]{1,0:T(8,128)(2,1)S(1)}, bf16[1024,128]{1,0:T(8,128)(2,1)S(1)}, u32[]{:S(2)}, u32[]{:S(2)}) collective-permute-start(bf16[1024,128]{1,0:T(8,128)(2,1)S(1)} %copy-done.1), channel_id=1, source_target_pairs={{0,2},{1,3},{2,0},{3,1},{4,6},{5,7},{6,4},{7,5},{8,10},{9,11},{10,... | collective-permute-start | bytes 786440 | tf_op jit(solution)/shard_map/ppermute | solution.py:214
  40.4 0.0 collective-permute-done.refs_1_
  40.4 2.1 %collective-permute-start.2 = (bf16[1024,128]{1,0:T(8,128)(2,1)S(1)}, bf16[1024,128]{1,0:T(8,128)(2,1)S(1)}, u32[]{:S(2)}, u32[]{:S(2)}) collective-permute-start(bf16[1024,128]{1,0:T(8,128)(2,1)S(1)} %collective-permute-done.refs_1_), channel_id=1, source_target_pairs={{0,2},{1,3},{2,0},{3,1},{4,6},{5,7},{6,4},{7,5},{8,10},{9,11},{10,... | collective-permute-start | bytes 786440 | tf_op jit(solution)/shard_map/ppermute | solution.py:214
  42.5 0.8 %all-to-all-done.1 = bf16[128,8,128]{2,1,0:T(8,128)(2,1)S(1)} async-done(((bf16[128,8,128]{2,1,0:T(8,128)(2,1)}), bf16[128,8,128]{2,1,0:T(8,128)(2,1)S(1)}, u32[]{:S(2)}, u32[]{:S(2)}) %all-to-all-start.1) | async-done | bytes 262176 | tf_op jit(solution)/shard_map/all_to_all | solution.py:222
  43.3 5.7 %all_gather.9.x_ref = bf16[2,64,2,8,128]{4,3,2,1,0:T(8,128)(2,1)S(1)} all-gather(bf16[1,64,2,8,128]{4,3,2,1,0:T(8,128)(2,1)S(1)} %bitcast.8), channel_id=1, replica_groups=mesh['row'=32,'g'=4,'h'=2,'k'=2] {'k'}, dimensions={0}, use_global_device_ids=true | all-gather | bytes 786432 | tf_op jit(solution)/shard_map/all_gather | solution.py:223
  49.0 0.0 copy-done
  49.0 0.6 shard_map.84
  49.6 15.1 %all-gather = bf16[1024,256]{1,0:T(8,128)(2,1)S(1)} all-gather(bf16[256,256]{1,0:T(8,128)(2,1)S(1)} %shard_map.84), channel_id=2, replica_groups=mesh['row'=32,'g'=4,'h'=2,'k'=2] {'g'}, dimensions={0}, use_global_device_ids=true | all-gather | bytes 655360 | tf_op jit(solution)/shard_map/all_gather | solution.py:226
  64.7 0.0 collective-permute-done.1.refs_2_
  64.7 0.0 collective-permute-done.2.refs_3_
  64.7 0.7 shard_map.85
  65.4 11.6 %all_to_all.16 = bf16[4,256,128]{2,1,0:T(8,128)(2,1)S(1)} all-to-all(bf16[4,256,128]{2,1,0:T(8,128)(2,1)S(1)} %shard_map.85), channel_id=1, replica_groups=mesh['row'=32,'g'=4,'h'=2,'k'=2] {'h','k'}, dimensions={0} | all-to-all | bytes 524288 | tf_op jit(solution)/shard_map/all_to_all | solution.py:229
  77.0 0.7 copy.10
Async XLA Ops:
  0.0 26.3 %copy-start.4 = (bf16[256,256]{1,0:T(8,128)(2,1)S(1)}, bf16[256,256]{1,0:T(8,128)(2,1)}, u32[]{:S(2)}) copy-start(bf16[256,256]{1,0:T(8,128)(2,1)} %constant.18.clone.two_ref) | copy-start | bytes 393220
  0.0 26.3 %copy-start.2 = (f32[2,256,128]{2,1,0:T(8,128)S(1)}, f32[2,256,128]{2,1,0:T(8,128)}, u32[]{:S(2)}) copy-start(f32[2,256,128]{2,1,0:T(8,128)} %constant.17.clone.turn_ref) | copy-start | bytes 786436
  0.0 26.3 %copy-start.3 = (bf16[512,256]{1,0:T(8,128)(2,1)S(1)}, bf16[512,256]{1,0:T(8,128)(2,1)}, u32[]{:S(2)}) copy-start(bf16[512,256]{1,0:T(8,128)(2,1)} %constant.16.clone.one_ref) | copy-start | bytes 786436
  0.0 49.0 %copy-start = (bf16[256,512]{1,0:T(8,128)(2,1)S(1)}, bf16[256,512]{1,0:T(8,128)(2,1)}, u32[]{:S(2)}) copy-start(bf16[256,512]{1,0:T(8,128)(2,1)} %constant.19.clone.table_ref) | copy-start | bytes 786436
  0.0 33.1 %copy-start.1 = (bf16[1024,128]{1,0:T(8,128)(2,1)S(1)}, bf16[1024,128]{1,0:T(8,128)(2,1)}, u32[]{:S(2)}) copy-start(bf16[1024,128]{1,0:T(8,128)(2,1)} %refs_0_.1) | copy-start | bytes 786436
  28.0 15.3 %all-to-all-start.1 = ((bf16[128,8,128]{2,1,0:T(8,128)(2,1)}), bf16[128,8,128]{2,1,0:T(8,128)(2,1)S(1)}, u32[]{:S(2)}, u32[]{:S(2)}) async-start(bf16[128,8,128]{2,1,0:T(8,128)(2,1)} %shard_map.83), calls=%async_computation.1 | async-start | bytes 524288 | tf_op jit(solution)/shard_map/all_to_all | solution.py:222
  33.1 7.2 %collective-permute-start = (bf16[1024,128]{1,0:T(8,128)(2,1)S(1)}, bf16[1024,128]{1,0:T(8,128)(2,1)S(1)}, u32[]{:S(2)}, u32[]{:S(2)}) collective-permute-start(bf16[1024,128]{1,0:T(8,128)(2,1)S(1)} %copy-done.1), channel_id=1, source_target_pairs={{0,1},{1,0},{2,3},{3,2},{4,5},{5,4},{6,7},{7,6},{8,9},{9,8},{10,11... | collective-permute-start | bytes 786440 | tf_op jit(solution)/shard_map/ppermute | solution.py:214
  37.1 27.5 %collective-permute-start.1 = (bf16[1024,128]{1,0:T(8,128)(2,1)S(1)}, bf16[1024,128]{1,0:T(8,128)(2,1)S(1)}, u32[]{:S(2)}, u32[]{:S(2)}) collective-permute-start(bf16[1024,128]{1,0:T(8,128)(2,1)S(1)} %copy-done.1), channel_id=1, source_target_pairs={{0,2},{1,3},{2,0},{3,1},{4,6},{5,7},{6,4},{7,5},{8,10},{9,11},{10,... | collective-permute-start | bytes 786440 | tf_op jit(solution)/shard_map/ppermute | solution.py:214
  40.4 24.3 %collective-permute-start.2 = (bf16[1024,128]{1,0:T(8,128)(2,1)S(1)}, bf16[1024,128]{1,0:T(8,128)(2,1)S(1)}, u32[]{:S(2)}, u32[]{:S(2)}) collective-permute-start(bf16[1024,128]{1,0:T(8,128)(2,1)S(1)} %collective-permute-done.refs_1_), channel_id=1, source_target_pairs={{0,2},{1,3},{2,0},{3,1},{4,6},{5,7},{6,4},{7,5},{8,10},{9,11},{10,... | collective-permute-start | bytes 786440 | tf_op jit(solution)/shard_map/ppermute | solution.py:214
